TPU v7x, 256 devices: a 4x2x16 block of a 4x16x16 slice. The times are simulated.
256 devices in a mesh: grp: 2 (over y), fs: 16 (over z), tp: 8 (over x, core).
Axes of the slice: x: 4, y: 2, z: 16, core: 2. Of those that a mesh axis runs over, the one named last changes fastest.
The devices are a block of a 4x16x16 slice.
Arguments:
- tokens: bfloat16 [128, 128, 2048], P(('grp', 'fs'), None, 'tp'), parts along dimension 0, may hold values from -100 to 100
- mix_gain: float32 [2048], replicated, may hold values from 0.1 to 1.9
- gate_outer: bfloat16 [2048, 1024], P('fs', 'tp'), may hold values from -0.125 to 0.125
- gate_inner: bfloat16 [2048, 1024], P('fs', 'tp'), may hold values from -0.125 to 0.125
- value_weight: bfloat16 [2048, 1024], P('fs', 'tp'), may hold values from -0.125 to 0.125
- conv_taps: float32 [3, 1024], replicated, may hold values from -3 to 3
- mix_out: bfloat16 [1024, 2048], P('tp', 'fs'), may hold values from -0.25 to 0.25
- ffn_gain: float32 [2048], replicated, may hold values from 0.1 to 1.9
- ffn_gate: bfloat16 [2048, 5632], P('fs', 'tp'), may hold values from -0.125 to 0.125
- ffn_up: bfloat16 [2048, 5632], P('fs', 'tp'), may hold values from -0.125 to 0.125
- ffn_down: bfloat16 [5632, 2048], P('tp', 'fs'), may hold values from -0.109375 to 0.109375
- out_gain: float32 [2048], replicated, may hold values from 0.1 to 1.9
Outputs:
- layer_out: bfloat16 [128, 128, 2048], P(('grp', 'fs'), None, 'tp'), parts along dimension 0
There are 2 independent parts, one for each index of `grp`. A program takes and returns all parts, laid end to end along the dimension named above; an argument that names none is the same for every part. Nothing has to cross between parts.
All inputs are finite; a program needn't handle non-finite values.
Results may differ from a plain program's by a relative error of at most 0.015.
Values may be sent and summed in bfloat16 or wider, within the bound.
No kernel may reach another device: no remote copies, remote signals or barrier semaphores. Data moves between devices by JAX's collectives and lax.ppermute only.
A program may use at most 64 MiB of HBM per device.

v0:
```python
import jax
import jax.numpy as jnp
from jax import lax
from jax.sharding import PartitionSpec as P


def in_order(parts, dim):
    parts = jnp.moveaxis(parts, 0, dim)
    shape = parts.shape
    return parts.reshape(*shape[:dim], shape[dim] * shape[dim + 1], *shape[dim + 2 :])


def copy_for_each(shard, axis):
    copies = jnp.broadcast_to(shard, (lax.axis_size(axis), *shard.shape))
    return lax.all_to_all(copies, axis, split_axis=0, concat_axis=0, tiled=True)


def collect(shard, axis, dim):
    return in_order(copy_for_each(shard, axis), dim)


def side_by_side(arrays, axis, dim, along):
    both = jnp.concatenate(arrays, axis=along)
    filled, at, outs = (lax.all_gather(both, axis, axis=dim, tiled=True), 0, [])
    for a in arrays:
        outs.append(lax.slice_in_dim(filled, at, at + a.shape[along], axis=along))
        at += a.shape[along]
    return tuple(outs)


def in_blocks(shard, dim, count):
    shape = shard.shape
    parts = shard.reshape(*shape[:dim], count, shape[dim] // count, *shape[dim + 1 :])
    return jnp.moveaxis(parts, dim, 0)


def summed_on_arrival(shard, axis, dim):
    parts = in_blocks(shard, dim, lax.axis_size(axis))
    arrived = lax.all_to_all(parts, axis, split_axis=0, concat_axis=0, tiled=True)
    return arrived.astype(jnp.float32).sum(axis=0)


def of_everyone(shard, axis):
    return copy_for_each(shard, axis).sum(axis=0)


def rms_norm(values, gain):
    floats = values.astype(jnp.float32)
    scaled = floats * lax.rsqrt(jnp.mean(floats * floats, axis=-1, keepdims=True) + 1e-06)
    return (scaled * gain).astype(jnp.bfloat16)


def local(
    tokens,
    mix_gain,
    gate_outer,
    gate_inner,
    value_weight,
    conv_taps,
    mix_out,
    ffn_gain,
    ffn_gate,
    ffn_up,
    ffn_down,
    out_gain,
):
    seq_count, length, columns = tokens.shape
    row_count = seq_count * length
    width = columns * lax.axis_size("tp")
    whole = collect(tokens, "tp", 2).reshape(row_count, width)
    normed = rms_norm(whole, mix_gain)
    channels = gate_outer.shape[1]
    pieces = side_by_side((gate_outer, gate_inner, value_weight), "fs", 0, 1)
    sliced = normed
    outer = jnp.dot(sliced, pieces[0], preferred_element_type=jnp.float32)
    inner = jnp.dot(sliced, pieces[1], preferred_element_type=jnp.float32)
    values = jnp.dot(sliced, pieces[2], preferred_element_type=jnp.float32)
    outer = outer.astype(jnp.bfloat16)
    inner = inner.astype(jnp.bfloat16)
    values = values.astype(jnp.bfloat16)
    product = (inner.astype(jnp.float32) * values.astype(jnp.float32)).reshape(
        seq_count, length, channels
    )
    own_taps = lax.dynamic_slice_in_dim(conv_taps, lax.axis_index("tp") * channels, channels, 1)
    tap_count = conv_taps.shape[0]
    padded = jnp.pad(product, ((0, 0), (tap_count - 1, 0), (0, 0)))
    conv = jnp.zeros((seq_count, length, channels), jnp.float32)
    for offset in range(tap_count):
        conv = conv + own_taps[offset] * padded[:, offset : offset + length]
    gated = (outer.astype(jnp.float32) * conv.reshape(row_count, channels)).astype(jnp.bfloat16)
    mix_terms = jnp.dot(gated, collect(mix_out, "fs", 1), preferred_element_type=jnp.float32)
    mix_summed = summed_on_arrival(mix_terms.astype(jnp.bfloat16), "tp", 1)
    first = (tokens.reshape(row_count, columns).astype(jnp.float32) + mix_summed).astype(
        jnp.bfloat16
    )
    whole_ffn = collect(first.reshape(seq_count, length, columns), "tp", 2).reshape(
        row_count, width
    )
    normed_ffn = rms_norm(whole_ffn, ffn_gain)
    pieces = side_by_side((ffn_gate, ffn_up), "fs", 0, 1)
    sliced = normed_ffn
    gate = jnp.dot(sliced, pieces[0], preferred_element_type=jnp.float32)
    upward = jnp.dot(sliced, pieces[1], preferred_element_type=jnp.float32)
    hidden = (jax.nn.silu(gate) * upward).astype(jnp.bfloat16)
    down_terms = jnp.dot(
        hidden,
        lax.all_gather(ffn_down, "fs", axis=1, tiled=True),
        preferred_element_type=jnp.float32,
    )
    down_summed = summed_on_arrival(down_terms.astype(jnp.bfloat16), "tp", 1)
    second = first.astype(jnp.float32) + down_summed
    squares = of_everyone(jnp.sum(second * second, axis=1), "tp")
    factor = lax.rsqrt(squares / width + 1e-06)
    own_gain = lax.dynamic_slice_in_dim(out_gain, lax.axis_index("tp") * columns, columns, 0)
    result = second * factor[:, None] * own_gain
    return result.astype(jnp.bfloat16).reshape(seq_count, length, columns)


def solution(mesh):
    in_specs = (
        P(("grp", "fs"), None, "tp"),
        P(),
        P("fs", "tp"),
        P("fs", "tp"),
        P("fs", "tp"),
        P(),
        P("tp", "fs"),
        P(),
        P("fs", "tp"),
        P("fs", "tp"),
        P("tp", "fs"),
        P(),
    )
    out_specs = P(("grp", "fs"), None, "tp")
    return jax.shard_map(local, mesh=mesh, in_specs=in_specs, out_specs=out_specs, check_vma=False)
```

profile of v0, /device:TPU:33, one launch (start us, length us, event | category | flops | bytes accessed | tf_op | source)
XLA Modules:
  0.0 347.9 jit_solution(9210337294262374817)
XLA Ops:
  6.6 1.5 pad_maximum_fusion.1
  8.0 0.1 all-gather.4.cloned.1.call-update
  8.1 0.1 all-gather.6.cloned.1.call-start
  8.1 1.8 pad_maximum_fusion
  9.9 0.1 all-gather.6.cloned.1.call-update
  10.0 2.5 broadcast_in_dim.20
  12.5 24.1 %all-to-all-start = ((bf16[8,4,128,256]{3,2,1,0:T(8,128)(2,1)}), bf16[8,4,128,256]{3,2,1,0:T(8,128)(2,1)S(1)}, u32[]{:S(2)}, u32[]{:S(2)}) async-start(bf16[8,4,128,256]{3,2,1,0:T(8,128)(2,1)} %broadcast_in_dim.20), calls=%async_computation | async-start | bytes 4194304 | tf_op jit(solution)/shard_map/all_to_all | solution.py:15
  36.6 0.1 copy.25
  36.7 26.1 %all-to-all-done = bf16[8,4,128,256]{3,2,1,0:T(8,128)(2,1)S(1)} async-done(((bf16[8,4,128,256]{3,2,1,0:T(8,128)(2,1)}), bf16[8,4,128,256]{3,2,1,0:T(8,128)(2,1)S(1)}, u32[]{:S(2)}, u32[]{:S(2)}) %all-to-all-start) | async-done | bytes 2097184 | tf_op jit(solution)/shard_map/all_to_all | solution.py:15
  62.9 0.9 broadcast_in_dim.21
  63.7 5.7 %all-to-all-start.1 = ((bf16[16,128,128]{1,2,0:T(8,128)(2,1)}), bf16[16,128,128]{1,2,0:T(8,128)(2,1)S(1)}, u32[]{:S(2)}, u32[]{:S(2)}) async-start(bf16[16,128,128]{1,2,0:T(8,128)(2,1)} %broadcast_in_dim.21), calls=%async_computation.1 | async-start | bytes 1048576 | tf_op jit(solution)/shard_map/all_to_all | solution.py:15
  69.4 0.5 convert_bitcast_fusion.1
  70.0 2.4 copy.24
  72.4 2.0 copy.33
  74.4 0.0 copy-start.3
  74.4 0.5 fusion
  74.9 0.2 copy-done.3
  75.1 0.4 multiply_convert_fusion.1
  75.5 23.0 %all-gather.4.cloned.1.call-done = bf16[2048,384]{1,0:T(8,128)(2,1)} async-done(((bf16[128,384]{1,0:T(8,128)(2,1)}), bf16[2048,384]{1,0:T(8,128)(2,1)}) %all-gather.4.cloned.1.call-update) | async-done | bytes 1572880 | tf_op jit(solution)/shard_map/all_gather | solution.py:24
  98.4 1.7 fusion.14
  100.2 1.8 fusion.13
  102.0 0.1 fusion.27
  102.1 4.7 %convolution_convert_fusion = bf16[512,2048]{1,0:T(8,128)(2,1)} fusion(bf16[128,2048]{0,1:T(8,128)(2,1)S(1)} %bitcast.61, f32[512,128]{1,0:T(8,128)S(1)} %bitcast.63, bf16[512,2048]{1,0:T(8,128)(2,1)S(1)} %multiply_convert_fusion.1, bf16[2048,384]{1,0:T(8,128)(2,1)} %all-gather.4.cloned.1.call-done), kind=kOutput, calls=%fused_computation.10 | convolution fusion | flops 538181632 | bytes 5505024 | tf_op jit(solution)/shard_map/dot_general | solution.py:91
  106.7 3.1 copy.38
  109.8 13.0 %all-to-all-start.2 = ((bf16[8,512,256]{2,1,0:T(8,128)(2,1)}), bf16[8,512,256]{2,1,0:T(8,128)(2,1)S(1)}, u32[]{:S(2)}, u32[]{:S(2)}) async-start(bf16[8,512,256]{2,1,0:T(8,128)(2,1)} %bitcast.53), calls=%async_computation.2 | async-start | bytes 4194304 | tf_op jit(solution)/shard_map/all_to_all | solution.py:39
  122.9 0.7 all-gather.8.cloned.1.call-update
  123.6 25.4 %all-to-all-done.2 = bf16[8,512,256]{2,1,0:T(8,128)(2,1)S(1)} async-done(((bf16[8,512,256]{2,1,0:T(8,128)(2,1)}), bf16[8,512,256]{2,1,0:T(8,128)(2,1)S(1)}, u32[]{:S(2)}, u32[]{:S(2)}) %all-to-all-start.2) | async-done | bytes 2097184 | tf_op jit(solution)/shard_map/all_to_all | solution.py:39
  149.1 0.3 convert_reduce_fusion.1
  149.4 0.1 add_convert_fusion
  149.5 0.2 broadcast_in_dim.22
  149.7 29.7 %all_to_all.31 = bf16[8,4,128,256]{3,2,1,0:T(8,128)(2,1)S(1)} all-to-all(bf16[8,4,128,256]{3,2,1,0:T(8,128)(2,1)S(1)} %broadcast_in_dim.22), channel_id=1, replica_groups=mesh['grp'=2,'fs'=16,'tp'=8] {'tp'}, dimensions={0} | all-to-all | bytes 4194304 | tf_op jit(solution)/shard_map/all_to_all | solution.py:15
  179.4 0.5 convert_bitcast_fusion
  179.9 2.4 copy.27
  182.3 4.0 %copy.34 = f32[64,8,8,256]{3,1,2,0:T(8,128)} copy(f32[64,8,8,256]{3,2,1,0:T(8,128)S(1)} %bitcast.52) | data formatting | bytes 8388608
  186.3 0.5 fusion.1
  186.8 13.6 %all-gather.6.cloned.1.call-done = bf16[2048,1408]{0,1:T(8,128)(2,1)} async-done(((bf16[128,1408]{0,1:T(8,128)(2,1)}), bf16[2048,1408]{0,1:T(8,128)(2,1)}) %all-gather.6.cloned.1.call-update) | async-done | bytes 5767184 | tf_op jit(solution)/shard_map/all_gather | solution.py:24
  200.4 6.0 %fusion.4 = f32[512,704]{0,1:T(8,128)} fusion(bf16[2048,1408]{0,1:T(8,128)(2,1)} %all-gather.6.cloned.1.call-done, f32[512,2048]{1,0:T(8,128)} %bitcast.57, f32[2048]{0:T(1024)S(1)} %copy-done.4, f32[512]{0:T(512)S(1)} %rsqrt_bitcast_fusion.1), kind=kOutput, calls=%fused_computation.14 | convolution fusion | flops 1479540736 | bytes 8529920 | tf_op jit(solution)/shard_map/dot_general | solution.py:102
  206.4 74.6 %all-gather.8.cloned.1.call-done = bf16[704,2048]{1,0:T(8,128)(2,1)} async-done(((bf16[704,128]{1,0:T(8,128)(2,1)}), bf16[704,2048]{1,0:T(8,128)(2,1)}) %all-gather.8.cloned.1.call-update) | async-done | bytes 2883600 | tf_op jit(solution)/shard_map/all_gather | solution.py:107
  281.0 7.8 %convolution_convert_fusion.1 = bf16[512,2048]{1,0:T(8,128)(2,1)S(1)} fusion(bf16[704,2048]{1,0:T(8,128)(2,1)} %all-gather.8.cloned.1.call-done, bf16[2048,1408]{0,1:T(8,128)(2,1)} %all-gather.6.cloned.1.call-done, f32[512,704]{0,1:T(8,128)} %fusion.4, f32[512,2048]{1,0:T(8,128)} %bitcast.58, f32[2048]{0:T(1024)S(1)} %copy-done.4, ...), kind=kOutput, calls=%fused_computation.11 | convolution fusion | flops 2959147008 | bytes 13510656 | tf_op jit(solution)/shard_map/dot_general | solution.py:105
  288.9 0.1 copy.37
  289.0 41.4 %all_to_all.32 = bf16[8,512,256]{2,1,0:T(8,128)(2,1)S(1)} all-to-all(bf16[8,512,256]{2,1,0:T(8,128)(2,1)S(1)} %bitcast.55), channel_id=1, replica_groups=mesh['grp'=2,'fs'=16,'tp'=8] {'tp'}, dimensions={0} | all-to-all | bytes 4194304 | tf_op jit(solution)/shard_map/all_to_all | solution.py:39
  330.4 0.3 convert_reduce_fusion
  330.7 0.1 multiply_reduce_fusion
  330.9 0.6 broadcast_in_dim.24
  331.5 4.3 %all-to-all-start.5 = ((f32[8,1,512]{2,1,0:T(1,128)}), f32[8,1,512]{2,1,0:T(1,128)S(1)}, u32[]{:S(2)}, u32[]{:S(2)}) async-start(f32[8,1,512]{2,1,0:T(1,128)} %broadcast_in_dim.24), calls=%async_computation.5 | async-start | bytes 32768 | tf_op jit(solution)/shard_map/all_to_all | solution.py:15
  335.8 0.8 dynamic_slice.7
  336.6 4.0 %all-to-all-done.5 = f32[8,1,512]{2,1,0:T(1,128)S(1)} async-done(((f32[8,1,512]{2,1,0:T(1,128)}), f32[8,1,512]{2,1,0:T(1,128)S(1)}, u32[]{:S(2)}, u32[]{:S(2)}) %all-to-all-start.5) | async-done | bytes 16416 | tf_op jit(solution)/shard_map/all_to_all | solution.py:15
  340.6 0.8 multiply_convert_fusion.2
  (17 shorter events, 0.1 us)
Async XLA Ops:
  6.5 30.1 %copy-start = (f32[3,1024]{1,0:T(4,128)S(1)}, f32[3,1024]{1,0:T(4,128)}, u32[]{:S(2)}) copy-start(f32[3,1024]{1,0:T(4,128)} %param.17) | copy-start | bytes 36868
  6.6 91.9 %all-gather.4.cloned.1.call-start = ((), (), s32[]{:S(2)}) async-start(), calls=%async_computation.6 | async-start | bytes 1671168 | tf_op jit(solution)/shard_map/all_gather | solution.py:24
  8.1 192.4 %all-gather.6.cloned.1.call-start = ((), (), s32[]{:S(2)}) async-start(), calls=%async_computation.7 | async-start | bytes 6127616 | tf_op jit(solution)/shard_map/all_gather | solution.py:24
  12.5 24.1 %copy-start.2 = (bf16[128,128]{1,0:T(8,128)(2,1)S(1)}, bf16[128,128]{1,0:T(8,128)(2,1)}, u32[]{:S(2)}) copy-start(bf16[128,128]{1,0:T(8,128)(2,1)} %param.18) | copy-start | bytes 98308
  12.5 50.4 %all-to-all-start = ((bf16[8,4,128,256]{3,2,1,0:T(8,128)(2,1)}), bf16[8,4,128,256]{3,2,1,0:T(8,128)(2,1)S(1)}, u32[]{:S(2)}, u32[]{:S(2)}) async-start(bf16[8,4,128,256]{3,2,1,0:T(8,128)(2,1)} %broadcast_in_dim.20), calls=%async_computation | async-start | bytes 4194304 | tf_op jit(solution)/shard_map/all_to_all | solution.py:15
  63.7 38.3 %all-to-all-start.1 = ((bf16[16,128,128]{1,2,0:T(8,128)(2,1)}), bf16[16,128,128]{1,2,0:T(8,128)(2,1)S(1)}, u32[]{:S(2)}, u32[]{:S(2)}) async-start(bf16[16,128,128]{1,2,0:T(8,128)(2,1)} %broadcast_in_dim.21), calls=%async_computation.1 | async-start | bytes 1048576 | tf_op jit(solution)/shard_map/all_to_all | solution.py:15
  74.4 0.7 copy-start.3
  109.8 39.2 %all-to-all-start.2 = ((bf16[8,512,256]{2,1,0:T(8,128)(2,1)}), bf16[8,512,256]{2,1,0:T(8,128)(2,1)S(1)}, u32[]{:S(2)}, u32[]{:S(2)}) async-start(bf16[8,512,256]{2,1,0:T(8,128)(2,1)} %bitcast.53), calls=%async_computation.2 | async-start | bytes 4194304 | tf_op jit(solution)/shard_map/all_to_all | solution.py:39
  122.9 26.5 %copy-start.1 = (bf16[4,128,256]{2,1,0:T(8,128)(2,1)S(1)}, bf16[4,128,256]{2,1,0:T(8,128)(2,1)}, u32[]{:S(2)}) copy-start(bf16[4,128,256]{2,1,0:T(8,128)(2,1)} %param.12) | copy-start | bytes 786436
  122.9 158.1 %all-gather.8.cloned.1.call-start = ((), (), s32[]{:S(2)}) async-start(), calls=%async_computation.8 | async-start | bytes 3063808 | tf_op jit(solution)/shard_map/all_gather | solution.py:107
  186.3 14.1 %copy-start.4 = (f32[2048]{0:T(1024)S(1)}, f32[2048]{0:T(1024)}, u32[]{:S(2)}) copy-start(f32[2048]{0:T(1024)} %param.19) | copy-start | bytes 24580
  331.5 9.0 %all-to-all-start.5 = ((f32[8,1,512]{2,1,0:T(1,128)}), f32[8,1,512]{2,1,0:T(1,128)S(1)}, u32[]{:S(2)}, u32[]{:S(2)}) async-start(f32[8,1,512]{2,1,0:T(1,128)} %broadcast_in_dim.24), calls=%async_computation.5 | async-start | bytes 32768 | tf_op jit(solution)/shard_map/all_to_all | solution.py:15
Sparse Core Ops, SparseCore 0:
  9.1 89.2 all-gather.3
  100.2 100.1 all-gather.5
  202.2 78.7 all-gather.7
where the time goes:
time: 349 us; the launch traced here: 348 us
  waiting for transfers between devices  168 us (48%)
  blocking collectives  71.1 us (20%)
  starting transfers between devices  47.1 us (13%)
  matrix products  22 us (6%)
  local copies, waits for them, and re-layouts  19.4 us (6%)
  between operations  13.3 us (4%)
  other arithmetic  7.44 us (2%)
    all_gather x1, waiting for transfers between devices, local(): lax.all_gather(ffn_down, 'fs', axis=1, tiled=True)  74.6 us
    all_to_all x1, blocking collectives, summed_on_arrival(): lax.all_to_all(parts, axis, split_axis=0, concat_axis=0, tiled=True)  41.4 us
    all_gather x2, waiting for transfers between devices, side_by_side(): filled, at, outs = (lax.all_gather(both, axis, axis=dim, tiled=True), 0, [])  36.6 us
    all_to_all x3, starting transfers between devices, copy_for_each(): return lax.all_to_all(copies, axis, split_axis=0, concat_axis=0, tiled=True)  34 us
    all_to_all x3, waiting for transfers between devices, copy_for_each(): return lax.all_to_all(copies, axis, split_axis=0, concat_axis=0, tiled=True)  30.1 us
    all_to_all x1, blocking collectives, copy_for_each(): return lax.all_to_all(copies, axis, split_axis=0, concat_axis=0, tiled=True)  29.7 us
    all_to_all x1, waiting for transfers between devices, summed_on_arrival(): lax.all_to_all(parts, axis, split_axis=0, concat_axis=0, tiled=True)  25.4 us
    all_to_all x1, starting transfers between devices, summed_on_arrival(): lax.all_to_all(parts, axis, split_axis=0, concat_axis=0, tiled=True)  13 us
  transfers between devices with their start and end apart: 7, of which 6 were waited for; matrix products, arithmetic and copies ran while one was open for 11% of the time, Pallas kernels for 0%

commit v1 on v0

--- a/solution.py
+++ b/solution.py
@@ -1,7 +1,35 @@
+import functools
 import jax
 import jax.numpy as jnp
 from jax import lax
 from jax.sharding import PartitionSpec as P
+
+
+def begin_the_zones(here_x, bus_axis, join_dim):
+    a_next = lax.axis_size(bus_axis)
+    found_now, z_new, arr_now = (a_next, lax.axis_index(bus_axis), here_x.shape[join_dim])
+    by_place = tuple(((num, (num + 1) % found_now) for num in range(found_now)))
+    buffer = tuple(((num, (num - 1) % found_now) for num in range(found_now)))
+    r1 = jnp.zeros(
+        (*here_x.shape[:join_dim], found_now * arr_now, *here_x.shape[join_dim + 1 :]), here_x.dtype
+    )
+    r1 = lax.dynamic_update_slice_in_dim(r1, here_x, z_new * arr_now, axis=join_dim)
+    odd = right_arr = here_x
+    n_now = found_now // 2
+    for d in range(1, n_now + 1):
+        odd = lax.ppermute(odd, bus_axis, perm=by_place)
+        r1 = lax.dynamic_update_slice_in_dim(
+            r1, odd, (z_new - d) % found_now * arr_now, axis=join_dim
+        )
+        if d < found_now - n_now:
+            right_arr = lax.ppermute(right_arr, axis_name=bus_axis, perm=buffer)
+            r1 = lax.dynamic_update_slice_in_dim(
+                r1, right_arr, (z_new + d) % found_now * arr_now, axis=join_dim
+            )
+    return r1
+
+
+derive_edge_all = functools.partial(begin_the_zones, bus_axis="fs", join_dim=1)
 
 
 def in_order(parts, dim):
@@ -102,11 +130,7 @@
     gate = jnp.dot(sliced, pieces[0], preferred_element_type=jnp.float32)
     upward = jnp.dot(sliced, pieces[1], preferred_element_type=jnp.float32)
     hidden = (jax.nn.silu(gate) * upward).astype(jnp.bfloat16)
-    down_terms = jnp.dot(
-        hidden,
-        lax.all_gather(ffn_down, "fs", axis=1, tiled=True),
-        preferred_element_type=jnp.float32,
-    )
+    down_terms = jnp.dot(hidden, derive_edge_all(ffn_down), preferred_element_type=jnp.float32)
     down_summed = summed_on_arrival(down_terms.astype(jnp.bfloat16), "tp", 1)
     second = first.astype(jnp.float32) + down_summed
     squares = of_everyone(jnp.sum(second * second, axis=1), "tp")

time: 349 us -> 299 us (0.86)
  waiting for transfers between devices: 168 us -> 114 us
  blocking collectives: 71.1 us -> 39.2 us
  starting transfers between devices: 47.1 us -> 68.2 us
  local copies, waits for them, and re-layouts: 19.4 us -> 33.9 us
    all_gather x1 -> x0, waiting for transfers between devices: 74.6 us -> none  [local(): lax.all_gather(ffn_down, 'fs', axis=1, tiled=True)]
    ppermute x0 -> x15, waiting for transfers between devices: none -> 37.4 us  [the longest x8 25.4 us: begin_the_zones(): odd = lax.ppermute(odd, bus_axis, perm=by_place)]
    all_to_all x1 -> x0, blocking collectives: 29.7 us -> none  [copy_for_each(): return lax.all_to_all(copies, axis, split_axis=0, concat_axis=0, tiled=True)]
    ppermute x0 -> x15, starting transfers between devices: none -> 16.2 us  [the longest x7 11 us: begin_the_zones(): right_arr = lax.ppermute(right_arr, axis_name=bus_axis, perm=buffer)]
    all_gather x2, waiting for transfers between devices: 36.6 us -> 23 us  [side_by_side(): filled, at, outs = (lax.all_gather(both, axis, axis=dim, tiled=True), 0, [])]
    dynamic_update_slice x0 -> x16, local copies, waits for them, and re-layouts: none -> 11.3 us  [the longest x8 5.68 us: begin_the_zones(): lax.dynamic_update_slice_in_dim(r1, odd, (z_new - d) % found_now * arr_no...]
    all_to_all x3 -> x4, starting transfers between devices: 34 us -> 38.4 us  [copy_for_each(): return lax.all_to_all(copies, axis, split_axis=0, concat_axis=0, tiled=True)]
    all_to_all x3 -> x4, waiting for transfers between devices: 30.1 us -> 30.1 us  [copy_for_each(): return lax.all_to_all(copies, axis, split_axis=0, concat_axis=0, tiled=True)]
  transfers between devices with their start and end apart: 7 -> 22, of which waited for: 6 -> 16; matrix products, arithmetic and copies ran while one was open for 11% -> 15% of each run, Pallas kernels for 0% -> 0%
where the time goes in v1:
time: 299 us; the launch traced here: 298 us
  waiting for transfers between devices  114 us (38%)
  starting transfers between devices  68.2 us (23%)
  blocking collectives  39.2 us (13%)
  local copies, waits for them, and re-layouts  33.9 us (11%)
  matrix products  22 us (7%)
  between operations  13.7 us (5%)
  other arithmetic  7.43 us (2%)
    all_to_all x1, blocking collectives, summed_on_arrival(): lax.all_to_all(parts, axis, split_axis=0, concat_axis=0, tiled=True)  39.2 us
    all_to_all x4, starting transfers between devices, copy_for_each(): return lax.all_to_all(copies, axis, split_axis=0, concat_axis=0, tiled=True)  38.4 us
    all_to_all x4, waiting for transfers between devices, copy_for_each(): return lax.all_to_all(copies, axis, split_axis=0, concat_axis=0, tiled=True)  30.1 us
    ppermute x8, waiting for transfers between devices, begin_the_zones(): odd = lax.ppermute(odd, bus_axis, perm=by_place)  25.4 us
    all_to_all x1, waiting for transfers between devices, summed_on_arrival(): lax.all_to_all(parts, axis, split_axis=0, concat_axis=0, tiled=True)  23.5 us
    all_gather x2, waiting for transfers between devices, side_by_side(): filled, at, outs = (lax.all_gather(both, axis, axis=dim, tiled=True), 0, [])  23 us
    all_to_all x1, starting transfers between devices, summed_on_arrival(): lax.all_to_all(parts, axis, split_axis=0, concat_axis=0, tiled=True)  13.6 us
    ppermute x7, waiting for transfers between devices, begin_the_zones(): right_arr = lax.ppermute(right_arr, axis_name=bus_axis, perm=buffer)  12 us
  transfers between devices with their start and end apart: 22, of which 16 were waited for; matrix products, arithmetic and copies ran while one was open for 15% of the time, Pallas kernels for 0%

profile of v1, /device:TPU:33, one launch (start us, length us, event | category | flops | bytes accessed | tf_op | source)
XLA Modules:
  0.0 298.4 jit_solution(6325165433068159113)
XLA Ops:
  6.6 1.5 pad_maximum_fusion.1
  8.1 1.8 pad_maximum_fusion
  10.0 2.5 broadcast_in_dim.23
  12.5 23.9 %all-to-all-start = ((bf16[8,4,128,256]{3,2,1,0:T(8,128)(2,1)}), bf16[8,4,128,256]{3,2,1,0:T(8,128)(2,1)S(1)}, u32[]{:S(2)}, u32[]{:S(2)}) async-start(bf16[8,4,128,256]{3,2,1,0:T(8,128)(2,1)} %broadcast_in_dim.23), calls=%async_computation | async-start | bytes 4194304 | tf_op jit(solution)/shard_map/all_to_all | solution.py:43
  36.6 26.1 %all-to-all-done = bf16[8,4,128,256]{3,2,1,0:T(8,128)(2,1)S(1)} async-done(((bf16[8,4,128,256]{3,2,1,0:T(8,128)(2,1)}), bf16[8,4,128,256]{3,2,1,0:T(8,128)(2,1)S(1)}, u32[]{:S(2)}, u32[]{:S(2)}) %all-to-all-start) | async-done | bytes 2097184 | tf_op jit(solution)/shard_map/all_to_all | solution.py:43
  62.8 0.9 broadcast_in_dim.24
  63.7 5.7 %all-to-all-start.1 = ((bf16[16,128,128]{1,2,0:T(8,128)(2,1)}), bf16[16,128,128]{1,2,0:T(8,128)(2,1)S(1)}, u32[]{:S(2)}, u32[]{:S(2)}) async-start(bf16[16,128,128]{1,2,0:T(8,128)(2,1)} %broadcast_in_dim.24), calls=%async_computation.1 | async-start | bytes 1048576 | tf_op jit(solution)/shard_map/all_to_all | solution.py:43
  69.9 2.4 copy.24
  72.3 2.0 copy.33
  75.2 23.0 %all-gather.3.cloned.1.call-done = bf16[2048,384]{1,0:T(8,128)(2,1)} async-done(((bf16[128,384]{1,0:T(8,128)(2,1)}), bf16[2048,384]{1,0:T(8,128)(2,1)}) %all-gather.3.cloned.1.call-update) | async-done | bytes 1572880 | tf_op jit(solution)/shard_map/all_gather | solution.py:52
  98.2 1.7 fusion.14
  99.9 1.8 fusion.13
  101.8 4.7 %convolution_convert_fusion = bf16[512,2048]{1,0:T(8,128)(2,1)} fusion(bf16[128,2048]{0,1:T(8,128)(2,1)S(1)} %bitcast.61, f32[512,128]{1,0:T(8,128)S(1)} %bitcast.63, bf16[512,2048]{1,0:T(8,128)(2,1)S(1)} %multiply_convert_fusion.1, bf16[2048,384]{1,0:T(8,128)(2,1)} %all-gather.3.cloned.1.call-done), kind=kOutput, calls=%fused_computation.10 | convolution fusion | flops 538181632 | bytes 5505024 | tf_op jit(solution)/shard_map/dot_general | solution.py:119
  106.4 3.1 %copy.38 = bf16[64,8,8,256]{3,2,0,1:T(8,128)(2,1)} copy(bf16[64,8,8,256]{3,2,1,0:T(8,128)(2,1)} %bitcast.54) | data formatting | bytes 4194304 | tf_op jit(solution)/shard_map/reshape | solution.py:61
  109.6 13.6 %all-to-all-start.2 = ((bf16[8,512,256]{2,1,0:T(8,128)(2,1)}), bf16[8,512,256]{2,1,0:T(8,128)(2,1)S(1)}, u32[]{:S(2)}, u32[]{:S(2)}) async-start(bf16[8,512,256]{2,1,0:T(8,128)(2,1)} %bitcast.53), calls=%async_computation.2 | async-start | bytes 4194304 | tf_op jit(solution)/shard_map/all_to_all | solution.py:67
  123.4 2.5 collective-permute-start.1
  125.8 23.5 %all-to-all-done.2 = bf16[8,512,256]{2,1,0:T(8,128)(2,1)S(1)} async-done(((bf16[8,512,256]{2,1,0:T(8,128)(2,1)}), bf16[8,512,256]{2,1,0:T(8,128)(2,1)S(1)}, u32[]{:S(2)}, u32[]{:S(2)}) %all-to-all-start.2) | async-done | bytes 2097184 | tf_op jit(solution)/shard_map/all_to_all | solution.py:67
  149.7 1.6 broadcast_in_dim.25
  151.3 4.5 %all-to-all-start.3 = ((bf16[8,4,128,256]{3,2,1,0:T(8,128)(2,1)}), bf16[8,4,128,256]{3,2,1,0:T(8,128)(2,1)S(1)}, u32[]{:S(2)}, u32[]{:S(2)}) async-start(bf16[8,4,128,256]{3,2,1,0:T(8,128)(2,1)} %broadcast_in_dim.25), calls=%async_computation.3 | async-start | bytes 4194304 | tf_op jit(solution)/shard_map/all_to_all | solution.py:43
  155.8 2.0 broadcast_in_dim.26
  158.7 2.4 collective-permute-start.3
  162.5 6.3 %collective-permute-done.2 = bf16[704,128]{1,0:T(8,128)(2,1)S(1)} collective-permute-done((bf16[704,128]{1,0:T(8,128)(2,1)S(1)}, bf16[704,128]{1,0:T(8,128)(2,1)S(1)}, u32[]{:S(2)}, u32[]{:S(2)}) %collective-permute-start.2) | collective-permute-done | bytes 180256 | tf_op jit(solution)/shard_map/ppermute | solution.py:20
  168.8 2.7 collective-permute-start.5
  172.9 2.6 collective-permute-done.4
  175.5 2.3 collective-permute-start.6
  178.3 1.6 collective-permute-start.7
  180.6 0.7 constant_dynamic-update-slice_fusion.9
  181.3 2.7 collective-permute-done.6
  184.1 1.4 collective-permute-start.8
  185.5 2.2 collective-permute-done.7
  189.2 2.3 collective-permute-done.8
  191.5 0.9 collective-permute-start.10
  192.4 4.7 %collective-permute-done.9 = bf16[704,128]{1,0:T(8,128)(2,1)S(1)} collective-permute-done((bf16[704,128]{1,0:T(8,128)(2,1)S(1)}, bf16[704,128]{1,0:T(8,128)(2,1)S(1)}, u32[]{:S(2)}, u32[]{:S(2)}) %collective-permute-start.9) | collective-permute-done | bytes 180256 | tf_op jit(solution)/shard_map/ppermute | solution.py:25
  198.6 1.9 collective-permute-done.10
  200.6 3.7 %collective-permute-done.11 = bf16[704,128]{1,0:T(8,128)(2,1)S(1)} collective-permute-done((bf16[704,128]{1,0:T(8,128)(2,1)S(1)}, bf16[704,128]{1,0:T(8,128)(2,1)S(1)}, u32[]{:S(2)}, u32[]{:S(2)}) %collective-permute-start.11) | collective-permute-done | bytes 180256 | tf_op jit(solution)/shard_map/ppermute | solution.py:25
  204.3 1.7 collective-permute-start.13
  207.4 3.1 %collective-permute-done.12 = bf16[704,128]{1,0:T(8,128)(2,1)S(1)} collective-permute-done((bf16[704,128]{1,0:T(8,128)(2,1)S(1)}, bf16[704,128]{1,0:T(8,128)(2,1)S(1)}, u32[]{:S(2)}, u32[]{:S(2)}) %collective-permute-start.12) | collective-permute-done | bytes 180256 | tf_op jit(solution)/shard_map/ppermute | solution.py:20
  211.2 0.9 collective-permute-done.13
  212.8 6.5 %collective-permute-done.14 = bf16[704,128]{1,0:T(8,128)(2,1)S(1)} collective-permute-done((bf16[704,128]{1,0:T(8,128)(2,1)S(1)}, bf16[704,128]{1,0:T(8,128)(2,1)S(1)}, u32[]{:S(2)}, u32[]{:S(2)}) %collective-permute-start.14) | collective-permute-done | bytes 180256 | tf_op jit(solution)/shard_map/ppermute | solution.py:20
  220.5 2.4 copy.27
  223.0 4.0 %copy.34 = f32[64,8,8,256]{3,1,2,0:T(8,128)} copy(f32[64,8,8,256]{3,2,1,0:T(8,128)S(1)} %bitcast.52) | data formatting | bytes 8388608
  227.5 6.0 %fusion.4 = f32[512,704]{0,1:T(8,128)} fusion(bf16[2048,1408]{0,1:T(8,128)(2,1)} %all-gather.5.cloned.1.call-done, f32[512,2048]{1,0:T(8,128)} %bitcast.57, f32[2048]{0:T(1024)S(1)} %copy-done.6, f32[512]{0:T(512)S(1)} %rsqrt_bitcast_fusion.1), kind=kOutput, calls=%fused_computation.14 | convolution fusion | flops 1479540736 | bytes 8529920 | tf_op jit(solution)/shard_map/dot_general | solution.py:130
  233.5 7.8 %convolution_convert_fusion.1 = bf16[512,2048]{1,0:T(8,128)(2,1)S(1)} fusion(bf16[704,2048]{1,0:T(8,128)(2,1)} %constant_dynamic-update-slice_fusion, bf16[2048,1408]{0,1:T(8,128)(2,1)} %all-gather.5.cloned.1.call-done, f32[512,704]{0,1:T(8,128)} %fusion.4, f32[512,2048]{1,0:T(8,128)} %bitcast.58, f32[2048]{0:T(1024)S(1)} %copy-done.6, ...), kind=kOutput, calls=%fused_computation.11 | convolution fusion | flops 2959147008 | bytes 13510656 | tf_op jit(solution)/shard_map/dot_general | solution.py:133
  241.5 39.2 %all_to_all.31 = bf16[8,512,256]{2,1,0:T(8,128)(2,1)S(1)} all-to-all(bf16[8,512,256]{2,1,0:T(8,128)(2,1)S(1)} %bitcast.55), channel_id=1, replica_groups=mesh['grp'=2,'fs'=16,'tp'=8] {'tp'}, dimensions={0} | all-to-all | bytes 4194304 | tf_op jit(solution)/shard_map/all_to_all | solution.py:67
  281.7 4.3 %all-to-all-start.5 = ((f32[8,1,512]{2,1,0:T(1,128)}), f32[8,1,512]{2,1,0:T(1,128)S(1)}, u32[]{:S(2)}, u32[]{:S(2)}) async-start(f32[8,1,512]{2,1,0:T(1,128)} %broadcast_in_dim.28), calls=%async_computation.5 | async-start | bytes 32768 | tf_op jit(solution)/shard_map/all_to_all | solution.py:43
  286.0 0.8 dynamic_slice.7
  286.8 4.0 %all-to-all-done.5 = f32[8,1,512]{2,1,0:T(1,128)S(1)} async-done(((f32[8,1,512]{2,1,0:T(1,128)}), f32[8,1,512]{2,1,0:T(1,128)S(1)}, u32[]{:S(2)}, u32[]{:S(2)}) %all-to-all-start.5) | async-done | bytes 16416 | tf_op jit(solution)/shard_map/all_to_all | solution.py:43
  290.7 0.8 multiply_convert_fusion.2
  (66 shorter events, 16.2 us)
Async XLA Ops:
  6.5 30.0 %copy-start = (f32[3,1024]{1,0:T(4,128)S(1)}, f32[3,1024]{1,0:T(4,128)}, u32[]{:S(2)}) copy-start(f32[3,1024]{1,0:T(4,128)} %param.17) | copy-start | bytes 36868
  6.6 91.6 %all-gather.3.cloned.1.call-start = ((), (), s32[]{:S(2)}) async-start(), calls=%async_computation.6 | async-start | bytes 1671168 | tf_op jit(solution)/shard_map/all_gather | solution.py:52
  8.1 219.4 %all-gather.5.cloned.1.call-start = ((), (), s32[]{:S(2)}) async-start(), calls=%async_computation.7 | async-start | bytes 6127616 | tf_op jit(solution)/shard_map/all_gather | solution.py:52
  10.0 26.5 %copy-start.4 = (bf16[128,128]{1,0:T(8,128)(2,1)S(1)}, bf16[128,128]{1,0:T(8,128)(2,1)}, u32[]{:S(2)}) copy-start(bf16[128,128]{1,0:T(8,128)(2,1)} %param.18) | copy-start | bytes 98308
  12.5 50.2 %all-to-all-start = ((bf16[8,4,128,256]{3,2,1,0:T(8,128)(2,1)}), bf16[8,4,128,256]{3,2,1,0:T(8,128)(2,1)S(1)}, u32[]{:S(2)}, u32[]{:S(2)}) async-start(bf16[8,4,128,256]{3,2,1,0:T(8,128)(2,1)} %broadcast_in_dim.23), calls=%async_computation | async-start | bytes 4194304 | tf_op jit(solution)/shard_map/all_to_all | solution.py:43
  63.7 38.1 %all-to-all-start.1 = ((bf16[16,128,128]{1,2,0:T(8,128)(2,1)}), bf16[16,128,128]{1,2,0:T(8,128)(2,1)S(1)}, u32[]{:S(2)}, u32[]{:S(2)}) async-start(bf16[16,128,128]{1,2,0:T(8,128)(2,1)} %broadcast_in_dim.24), calls=%async_computation.1 | async-start | bytes 1048576 | tf_op jit(solution)/shard_map/all_to_all | solution.py:43
  72.3 2.5 copy-start.5
  109.6 13.6 %copy-start.3 = (bf16[704,128]{1,0:T(8,128)(2,1)S(1)}, bf16[704,128]{1,0:T(8,128)(2,1)}, u32[]{:S(2)}) copy-start(bf16[704,128]{1,0:T(8,128)(2,1)} %param.22) | copy-start | bytes 540676
  109.6 40.1 %copy-start.2 = (bf16[4,128,256]{2,1,0:T(8,128)(2,1)S(1)}, bf16[4,128,256]{2,1,0:T(8,128)(2,1)}, u32[]{:S(2)}) copy-start(bf16[4,128,256]{2,1,0:T(8,128)(2,1)} %param.12) | copy-start | bytes 786436
  109.6 39.8 %all-to-all-start.2 = ((bf16[8,512,256]{2,1,0:T(8,128)(2,1)}), bf16[8,512,256]{2,1,0:T(8,128)(2,1)S(1)}, u32[]{:S(2)}, u32[]{:S(2)}) async-start(bf16[8,512,256]{2,1,0:T(8,128)(2,1)} %bitcast.53), calls=%async_computation.2 | async-start | bytes 4194304 | tf_op jit(solution)/shard_map/all_to_all | solution.py:67
  123.1 35.3 %collective-permute-start = (bf16[704,128]{1,0:T(8,128)(2,1)S(1)}, bf16[704,128]{1,0:T(8,128)(2,1)S(1)}, u32[]{:S(2)}, u32[]{:S(2)}) collective-permute-start(bf16[704,128]{1,0:T(8,128)(2,1)S(1)} %copy-done.3), channel_id=1, source_target_pairs={{0,8},{8,16},{16,24},{24,32},{32,40},{40,48},{48,56},{56,64},{64,7... | collective-permute-start | bytes 540680 | tf_op jit(solution)/shard_map/ppermute | solution.py:20
  123.4 35.3 %collective-permute-start.1 = (bf16[704,128]{1,0:T(8,128)(2,1)S(1)}, bf16[704,128]{1,0:T(8,128)(2,1)S(1)}, u32[]{:S(2)}, u32[]{:S(2)}) collective-permute-start(bf16[704,128]{1,0:T(8,128)(2,1)S(1)} %copy-done.3), channel_id=1, source_target_pairs={{0,120},{8,0},{16,8},{24,16},{32,24},{40,32},{48,40},{56,48},{64,5... | collective-permute-start | bytes 540680 | tf_op jit(solution)/shard_map/ppermute | solution.py:25
  151.3 68.7 %all-to-all-start.3 = ((bf16[8,4,128,256]{3,2,1,0:T(8,128)(2,1)}), bf16[8,4,128,256]{3,2,1,0:T(8,128)(2,1)S(1)}, u32[]{:S(2)}, u32[]{:S(2)}) async-start(bf16[8,4,128,256]{3,2,1,0:T(8,128)(2,1)} %broadcast_in_dim.25), calls=%async_computation.3 | async-start | bytes 4194304 | tf_op jit(solution)/shard_map/all_to_all | solution.py:43
  158.4 10.4 %collective-permute-start.2 = (bf16[704,128]{1,0:T(8,128)(2,1)S(1)}, bf16[704,128]{1,0:T(8,128)(2,1)S(1)}, u32[]{:S(2)}, u32[]{:S(2)}) collective-permute-start(bf16[704,128]{1,0:T(8,128)(2,1)S(1)} %collective-permute-done), channel_id=1, source_target_pairs={{0,8},{8,16},{16,24},{24,32},{32,40},{40,48},{48,56},{56,64},{64,7... | collective-permute-start | bytes 540680 | tf_op jit(solution)/shard_map/ppermute | solution.py:20
  158.7 10.2 %collective-permute-start.3 = (bf16[704,128]{1,0:T(8,128)(2,1)S(1)}, bf16[704,128]{1,0:T(8,128)(2,1)S(1)}, u32[]{:S(2)}, u32[]{:S(2)}) collective-permute-start(bf16[704,128]{1,0:T(8,128)(2,1)S(1)} %collective-permute-done.1), channel_id=1, source_target_pairs={{0,120},{8,0},{16,8},{24,16},{32,24},{40,32},{48,40},{56,48},{64,5... | collective-permute-start | bytes 540680 | tf_op jit(solution)/shard_map/ppermute | solution.py:25
  168.8 6.6 %collective-permute-start.4 = (bf16[704,128]{1,0:T(8,128)(2,1)S(1)}, bf16[704,128]{1,0:T(8,128)(2,1)S(1)}, u32[]{:S(2)}, u32[]{:S(2)}) collective-permute-start(bf16[704,128]{1,0:T(8,128)(2,1)S(1)} %collective-permute-done.2), channel_id=1, source_target_pairs={{0,8},{8,16},{16,24},{24,32},{32,40},{40,48},{48,56},{56,64},{64,7... | collective-permute-start | bytes 540680 | tf_op jit(solution)/shard_map/ppermute | solution.py:20
  168.8 9.4 %collective-permute-start.5 = (bf16[704,128]{1,0:T(8,128)(2,1)S(1)}, bf16[704,128]{1,0:T(8,128)(2,1)S(1)}, u32[]{:S(2)}, u32[]{:S(2)}) collective-permute-start(bf16[704,128]{1,0:T(8,128)(2,1)S(1)} %collective-permute-done.3), channel_id=1, source_target_pairs={{0,120},{8,0},{16,8},{24,16},{32,24},{40,32},{48,40},{56,48},{64,5... | collective-permute-start | bytes 540680 | tf_op jit(solution)/shard_map/ppermute | solution.py:25
  175.5 8.6 %collective-permute-start.6 = (bf16[704,128]{1,0:T(8,128)(2,1)S(1)}, bf16[704,128]{1,0:T(8,128)(2,1)S(1)}, u32[]{:S(2)}, u32[]{:S(2)}) collective-permute-start(bf16[704,128]{1,0:T(8,128)(2,1)S(1)} %collective-permute-done.4), channel_id=1, source_target_pairs={{0,8},{8,16},{16,24},{24,32},{32,40},{40,48},{48,56},{56,64},{64,7... | collective-permute-start | bytes 540680 | tf_op jit(solution)/shard_map/ppermute | solution.py:20
  178.3 9.5 %collective-permute-start.7 = (bf16[704,128]{1,0:T(8,128)(2,1)S(1)}, bf16[704,128]{1,0:T(8,128)(2,1)S(1)}, u32[]{:S(2)}, u32[]{:S(2)}) collective-permute-start(bf16[704,128]{1,0:T(8,128)(2,1)S(1)} %collective-permute-done.5), channel_id=1, source_target_pairs={{0,120},{8,0},{16,8},{24,16},{32,24},{40,32},{48,40},{56,48},{64,5... | collective-permute-start | bytes 540680 | tf_op jit(solution)/shard_map/ppermute | solution.py:25
  184.1 7.4 %collective-permute-start.8 = (bf16[704,128]{1,0:T(8,128)(2,1)S(1)}, bf16[704,128]{1,0:T(8,128)(2,1)S(1)}, u32[]{:S(2)}, u32[]{:S(2)}) collective-permute-start(bf16[704,128]{1,0:T(8,128)(2,1)S(1)} %collective-permute-done.6), channel_id=1, source_target_pairs={{0,8},{8,16},{16,24},{24,32},{32,40},{40,48},{48,56},{56,64},{64,7... | collective-permute-start | bytes 540680 | tf_op jit(solution)/shard_map/ppermute | solution.py:20
  187.8 9.3 %collective-permute-start.9 = (bf16[704,128]{1,0:T(8,128)(2,1)S(1)}, bf16[704,128]{1,0:T(8,128)(2,1)S(1)}, u32[]{:S(2)}, u32[]{:S(2)}) collective-permute-start(bf16[704,128]{1,0:T(8,128)(2,1)S(1)} %collective-permute-done.7), channel_id=1, source_target_pairs={{0,120},{8,0},{16,8},{24,16},{32,24},{40,32},{48,40},{56,48},{64,5... | collective-permute-start | bytes 540680 | tf_op jit(solution)/shard_map/ppermute | solution.py:25
  191.5 9.0 %collective-permute-start.10 = (bf16[704,128]{1,0:T(8,128)(2,1)S(1)}, bf16[704,128]{1,0:T(8,128)(2,1)S(1)}, u32[]{:S(2)}, u32[]{:S(2)}) collective-permute-start(bf16[704,128]{1,0:T(8,128)(2,1)S(1)} %collective-permute-done.8), channel_id=1, source_target_pairs={{0,8},{8,16},{16,24},{24,32},{32,40},{40,48},{48,56},{56,64},{64,7... | collective-permute-start | bytes 540680 | tf_op jit(solution)/shard_map/ppermute | solution.py:20
  197.1 7.2 %collective-permute-start.11 = (bf16[704,128]{1,0:T(8,128)(2,1)S(1)}, bf16[704,128]{1,0:T(8,128)(2,1)S(1)}, u32[]{:S(2)}, u32[]{:S(2)}) collective-permute-start(bf16[704,128]{1,0:T(8,128)(2,1)S(1)} %collective-permute-done.9), channel_id=1, source_target_pairs={{0,120},{8,0},{16,8},{24,16},{32,24},{40,32},{48,40},{56,48},{64,5... | collective-permute-start | bytes 540680 | tf_op jit(solution)/shard_map/ppermute | solution.py:25
  200.5 10.0 %collective-permute-start.12 = (bf16[704,128]{1,0:T(8,128)(2,1)S(1)}, bf16[704,128]{1,0:T(8,128)(2,1)S(1)}, u32[]{:S(2)}, u32[]{:S(2)}) collective-permute-start(bf16[704,128]{1,0:T(8,128)(2,1)S(1)} %collective-permute-done.10), channel_id=1, source_target_pairs={{0,8},{8,16},{16,24},{24,32},{32,40},{40,48},{48,56},{56,64},{64,7... | collective-permute-start | bytes 540680 | tf_op jit(solution)/shard_map/ppermute | solution.py:20
  204.3 7.8 %collective-permute-start.13 = (bf16[704,128]{1,0:T(8,128)(2,1)S(1)}, bf16[704,128]{1,0:T(8,128)(2,1)S(1)}, u32[]{:S(2)}, u32[]{:S(2)}) collective-permute-start(bf16[704,128]{1,0:T(8,128)(2,1)S(1)} %collective-permute-done.11), channel_id=1, source_target_pairs={{0,120},{8,0},{16,8},{24,16},{32,24},{40,32},{48,40},{56,48},{64,5... | collective-permute-start | bytes 540680 | tf_op jit(solution)/shard_map/ppermute | solution.py:25
  210.5 8.8 %collective-permute-start.14 = (bf16[704,128]{1,0:T(8,128)(2,1)S(1)}, bf16[704,128]{1,0:T(8,128)(2,1)S(1)}, u32[]{:S(2)}, u32[]{:S(2)}) collective-permute-start(bf16[704,128]{1,0:T(8,128)(2,1)S(1)} %collective-permute-done.12), channel_id=1, source_target_pairs={{0,8},{8,16},{16,24},{24,32},{32,40},{40,48},{48,56},{56,64},{64,7... | collective-permute-start | bytes 540680 | tf_op jit(solution)/shard_map/ppermute | solution.py:20
  223.0 4.5 %copy-start.6 = (f32[2048]{0:T(1024)S(1)}, f32[2048]{0:T(1024)}, u32[]{:S(2)}) copy-start(f32[2048]{0:T(1024)} %param.19) | copy-start | bytes 24580
  241.5 50.1 %copy-start.1 = (f32[3,1024]{1,0:T(4,128)S(1)}, f32[3,1024]{1,0:T(4,128)}, u32[]{:S(2)}) copy-start(f32[3,1024]{1,0:T(4,128)} %param.17) | copy-start | bytes 36868
  281.7 9.0 %all-to-all-start.5 = ((f32[8,1,512]{2,1,0:T(1,128)}), f32[8,1,512]{2,1,0:T(1,128)S(1)}, u32[]{:S(2)}, u32[]{:S(2)}) async-start(f32[8,1,512]{2,1,0:T(1,128)} %broadcast_in_dim.28), calls=%async_computation.5 | async-start | bytes 32768 | tf_op jit(solution)/shard_map/all_to_all | solution.py:43
Sparse Core Ops, SparseCore 0:
  9.1 88.9 all-gather.2
  99.9 121.5 all-gather.4
